TPU v7x, 256 devices: a whole 4x4x8 slice. The times are simulated.
256 devices in a mesh: fs: 32 (over z, y), tp: 8 (over x, core).
Axes of the slice: x: 4, y: 4, z: 8, core: 2. Of those that a mesh axis runs over, the one named last changes fastest.
Arguments:
- inputs: bfloat16 [65536, 2048], P('fs'), may hold values from -6 to 6
- cotangents: bfloat16 [3, 65536, 1024], P(None, 'fs', 'tp'), as said below
- factor: bfloat16 [2048, 256], P('fs'), as said below
- weights: float32 [3, 2048, 1024], P(None, 'fs', 'tp'), may hold values from -0.125 to 0.125
- first_moment: float32 [3, 256, 1024], P(None, 'fs', 'tp'), may hold values from -0.6 to 0.6
- second_moment: float32 [3, 256, 1024], P(None, 'fs', 'tp'), may hold values from 0.001 to 0.01
Outputs:
- update: float32 [3, 2048, 1024], P(None, 'fs', 'tp')
- new_weights: float32 [3, 2048, 1024], P(None, 'fs', 'tp')
- copies: bfloat16 [3, 2048, 1024], P(None, None, 'tp')
- new_first: float32 [3, 256, 1024], P(None, 'fs', 'tp')
- new_second: float32 [3, 256, 1024], P(None, 'fs', 'tp')
Inputs may be any that keep to these rules, and one draw needn't show every extreme that they name: A real-valued factor of full rank. real-valued cotangents.
All inputs are finite; a program needn't handle non-finite values.
Results may differ from a plain program's by a relative error of at most 0.0085.
Values may be sent and summed in bfloat16 or wider, within the bound.
No kernel may reach another device: no remote copies, remote signals or barrier semaphores. Data moves between devices by JAX's collectives and lax.ppermute only.
A program may use at most 64 MiB of HBM per device.

v0:
```python
import jax
import jax.numpy as jnp
from jax import lax
from jax.sharding import Mesh
from jax.sharding import PartitionSpec as P

MW = 1024
RANK = 256
FS = ("fs_0", "fs_1")
FS_TP = ("fs_0", "fs_1", "tp_0", "tp_1")
TP = ("tp_0", "tp_1")


def joined_along(blocks, dim):
    blocks = jnp.moveaxis(blocks, 0, dim)
    shape = blocks.shape
    return blocks.reshape(*shape[:dim], shape[dim] * shape[dim + 1], *shape[dim + 2 :])


def sent_to_all(array, axis):
    copies = jnp.broadcast_to(array, (lax.axis_size(axis), *array.shape))
    return lax.all_to_all(copies, axis, split_axis=0, concat_axis=0, tiled=True)


def collect(array, axis, dim):
    return joined_along(sent_to_all(array, axis), dim)


def split_up(array, dim, count):
    before, after = (array.shape[:dim], array.shape[dim + 1 :])
    return jnp.moveaxis(array.reshape(*before, count, -1, *after), dim, 0)


def sent_and_summed(array, axis, dim):
    blocks = split_up(array, dim, lax.axis_size(axis))
    arrived = lax.all_to_all(blocks, axis, split_axis=0, concat_axis=0, tiled=True)
    return arrived.sum(axis=0)


def over_axes(array, axes):
    for axis in axes:
        array = lax.psum(array, axis)
    return array


def on_device(inputs, cotangents, factor, weights, first_moment, second_moment):
    factor_wide = factor.astype(jnp.float32)
    local_gradient = jnp.einsum(
        "td,mtc->dmc", inputs, cotangents, preferred_element_type=jnp.float32
    )
    gradient_high = local_gradient.astype(jnp.bfloat16)
    gradient_low = (local_gradient - gradient_high.astype(jnp.float32)).astype(jnp.bfloat16)
    factor_piece = collect(factor, FS, 0)
    high_term = jnp.einsum(
        "dr,dmc->rmc", factor_piece, gradient_high, preferred_element_type=jnp.float32
    )
    low_term = jnp.einsum(
        "dr,dmc->rmc", factor_piece, gradient_low, preferred_element_type=jnp.float32
    )
    partial_value = high_term + low_term
    summed = sent_and_summed(partial_value, FS, 0)
    projected = jnp.transpose(summed, (1, 0, 2))
    square_sum = over_axes(jnp.sum(projected * projected), FS_TP)
    root_mean = jnp.sqrt(square_sum / (3 * RANK * MW) + 1e-06)
    clip_factor = jnp.minimum(1.0, 0.25 / root_mean)
    clipped = clip_factor * projected
    new_first = 0.9 * first_moment + 0.1 * clipped
    new_second = 0.95 * second_moment + 0.05 * clipped * clipped
    normed = new_first / (jnp.sqrt(new_second) + 1e-08)
    normed_whole = collect(normed, FS, 1)
    update = jnp.einsum("dr,mrc->mdc", factor_wide, normed_whole)
    new_weights = weights - 0.02 * update
    copies = collect(new_weights.astype(jnp.bfloat16), FS, 1)
    return (update, new_weights, copies, new_first, new_second)


def solution(mesh):
    torus = Mesh(mesh.devices.reshape(8, 4, 4, 2), ("fs_0", "fs_1", "tp_0", "tp_1"))
    return jax.shard_map(
        on_device,
        mesh=torus,
        in_specs=(
            P(FS, None),
            P(None, FS, TP),
            P(FS, None),
            P(None, FS, TP),
            P(None, FS, TP),
            P(None, FS, TP),
        ),
        out_specs=(
            P(None, FS, TP),
            P(None, FS, TP),
            P(None, None, TP),
            P(None, FS, TP),
            P(None, FS, TP),
        ),
        check_vma=False,
    )
```

profile of v0, /device:TPU:32, one launch (start us, length us, event | category | flops | bytes accessed | tf_op | source)
XLA Modules:
  0.0 169.0 jit_solution(2127882930247664799)
XLA Ops:
  0.6 0.0 copy-start
  0.6 2.0 %broadcast_in_dim.9 = bf16[32,64,256]{2,1,0:T(8,128)(2,1)} broadcast(bf16[64,256]{1,0:T(8,128)(2,1)} %param.8), dimensions={1,2} | broadcast | bytes 1081344 | tf_op jit(solution)/shard_map/broadcast_in_dim | solution.py:21
  2.6 11.4 %all-to-all-start = ((bf16[32,64,256]{2,1,0:T(8,128)(2,1)}), bf16[32,64,256]{2,1,0:T(8,128)(2,1)S(1)}, u32[]{:S(2)}, u32[]{:S(2)}) async-start(bf16[32,64,256]{2,1,0:T(8,128)(2,1)} %broadcast_in_dim.9), calls=%async_computation | async-start | bytes 2097152 | tf_op jit(solution)/shard_map/all_to_all | solution.py:22
  14.0 0.0 copy-done
  14.0 8.6 %fusion = f32[2048,3,128]{2,0,1:T(8,128)} fusion(bf16[3,2048,128]{2,1,0:T(8,128)(2,1)S(1)} %copy-done, bf16[2048,2048]{1,0:T(8,128)(2,1)} %param.6), kind=kOutput, calls=%fused_computation | convolution fusion | flops 3221225472 | bytes 13107200 | tf_op jit(solution)/shard_map/td,mtc->dmc/dot_general | solution.py:48
  22.6 18.5 %all-to-all-done = bf16[32,64,256]{2,1,0:T(8,128)(2,1)S(1)} async-done(((bf16[32,64,256]{2,1,0:T(8,128)(2,1)}), bf16[32,64,256]{2,1,0:T(8,128)(2,1)S(1)}, u32[]{:S(2)}, u32[]{:S(2)}) %all-to-all-start) | async-done | bytes 1048608 | tf_op jit(solution)/shard_map/all_to_all | solution.py:22
  41.2 0.0 copy-start.1
  41.2 2.7 %fusion.6 = f32[3,128,256]{2,1,0:T(8,128)S(1)} fusion(bf16[2048,256,1]{1,0,2:T(8,128)(2,1)S(1)} %bitcast.38, f32[2048,3,128]{2,0,1:T(8,128)} %fusion), kind=kOutput, calls=%fused_computation.8 | convolution fusion | flops 403439616 | bytes 4587520 | tf_op jit(solution)/shard_map/dr,dmc->rmc/dot_general | solution.py:54
  43.8 0.1 copy-done.1
  44.0 0.0 copy-start.4
  44.0 0.0 copy-start.5
  44.0 0.0 copy-start.2
  44.0 0.0 copy-start.3
  44.0 0.6 fusion.4
  44.7 0.2 copy.27
  44.9 19.9 %all_to_all.20 = f32[32,8,3,128]{3,1,2,0:T(8,128)S(1)} all-to-all(f32[32,8,3,128]{3,1,2,0:T(8,128)S(1)} %copy.28), channel_id=1, replica_groups=mesh['fs_0'=8,'fs_1'=4,'tp_0'=4,'tp_1'=2] {'fs_0','fs_1'}, dimensions={0} | all-to-all | bytes 786432 | tf_op jit(solution)/shard_map/all_to_all | solution.py:36
  64.8 0.6 multiply_reduce_fusion
  65.4 15.6 %psum.28 = f32[]{:T(128)} all-reduce(f32[]{:T(128)} %multiply_reduce_fusion), channel_id=1, replica_groups=mesh['fs_0'=8,'fs_1'=4,'tp_0'=4,'tp_1'=2] {'fs_0'}, use_global_device_ids=true, to_apply=%region_2.0 | all-reduce | flops 1 | bytes 8 | tf_op jit(solution)/shard_map/psum | solution.py:42
  81.0 10.1 %psum.29 = f32[]{:T(128)} all-reduce(f32[]{:T(128)} %psum.28), channel_id=1, replica_groups=mesh['fs_0'=8,'fs_1'=4,'tp_0'=4,'tp_1'=2] {'fs_1'}, use_global_device_ids=true, to_apply=%region_3.0 | all-reduce | flops 1 | bytes 8 | tf_op jit(solution)/shard_map/psum | solution.py:42
  91.0 11.1 %psum.30 = f32[]{:T(128)} all-reduce(f32[]{:T(128)} %psum.29), channel_id=1, replica_groups=mesh['fs_0'=8,'fs_1'=4,'tp_0'=4,'tp_1'=2] {'tp_0'}, use_global_device_ids=true, to_apply=%region_4.0 | all-reduce | flops 1 | bytes 8 | tf_op jit(solution)/shard_map/psum | solution.py:42
  102.1 3.1 %psum.31 = f32[]{:T(128)} all-reduce(f32[]{:T(128)} %psum.30), channel_id=1, replica_groups=mesh['fs_0'=8,'fs_1'=4,'tp_0'=4,'tp_1'=2] {'tp_1'}, use_global_device_ids=true, to_apply=%region_5.0 | all-reduce | flops 1 | bytes 8 | tf_op jit(solution)/shard_map/psum | solution.py:42
  105.9 0.0 copy-done.4
  105.9 0.0 copy-done.5
  105.9 0.6 add_divide_fusion
  106.6 16.5 %all_to_all.21 = bf16[32,3,8,128]{3,2,1,0:T(8,128)(2,1)S(1)} all-to-all(bf16[32,3,8,128]{3,2,1,0:T(8,128)(2,1)S(1)} %broadcast_in_dim.10), channel_id=1, replica_groups=mesh['fs_0'=8,'fs_1'=4,'tp_0'=4,'tp_1'=2] {'fs_0','fs_1'}, dimensions={0} | all-to-all | bytes 393216 | tf_op jit(solution)/shard_map/all_to_all | solution.py:22
  123.1 0.0 copy-done.2
  123.1 0.0 copy-done.3
  123.1 0.8 fusion.13
  123.9 0.4 broadcast_in_dim.11
  124.3 43.4 %all_to_all.22 = bf16[32,3,64,128]{3,2,1,0:T(8,128)(2,1)S(1)} all-to-all(bf16[32,3,64,128]{3,2,1,0:T(8,128)(2,1)S(1)} %broadcast_in_dim.11), channel_id=1, replica_groups=mesh['fs_0'=8,'fs_1'=4,'tp_0'=4,'tp_1'=2] {'fs_0','fs_1'}, dimensions={0} | all-to-all | bytes 3145728 | tf_op jit(solution)/shard_map/all_to_all | solution.py:22
  167.7 1.3 copy.30
  (3 shorter events, 0.1 us)
Async XLA Ops:
  0.6 13.4 %copy-start = (bf16[3,2048,128]{2,1,0:T(8,128)(2,1)S(1)}, bf16[3,2048,128]{2,1,0:T(8,128)(2,1)}, u32[]{:S(2)}) copy-start(bf16[3,2048,128]{2,1,0:T(8,128)(2,1)} %param.7) | copy-start | bytes 4718596
  2.6 38.5 %all-to-all-start = ((bf16[32,64,256]{2,1,0:T(8,128)(2,1)}), bf16[32,64,256]{2,1,0:T(8,128)(2,1)S(1)}, u32[]{:S(2)}, u32[]{:S(2)}) async-start(bf16[32,64,256]{2,1,0:T(8,128)(2,1)} %broadcast_in_dim.9), calls=%async_computation | async-start | bytes 2097152 | tf_op jit(solution)/shard_map/all_to_all | solution.py:22
  41.2 2.8 %copy-start.1 = (f32[2048,3,128]{2,0,1:T(8,128)S(1)}, f32[2048,3,128]{2,0,1:T(8,128)}, u32[]{:S(2)}) copy-start(f32[2048,3,128]{2,0,1:T(8,128)} %fusion) | copy-start | bytes 9437188
  44.0 61.9 %copy-start.4 = (f32[3,8,128]{2,1,0:T(8,128)S(1)}, f32[3,8,128]{2,1,0:T(8,128)}, u32[]{:S(2)}) copy-start(f32[3,8,128]{2,1,0:T(8,128)} %param.11) | copy-start | bytes 36868
  44.0 61.9 %copy-start.5 = (f32[3,8,128]{2,1,0:T(8,128)S(1)}, f32[3,8,128]{2,1,0:T(8,128)}, u32[]{:S(2)}) copy-start(f32[3,8,128]{2,1,0:T(8,128)} %param.10) | copy-start | bytes 36868
  44.0 79.1 %copy-start.2 = (bf16[64,256]{1,0:T(8,128)(2,1)S(1)}, bf16[64,256]{1,0:T(8,128)(2,1)}, u32[]{:S(2)}) copy-start(bf16[64,256]{1,0:T(8,128)(2,1)} %param.8) | copy-start | bytes 98308
  44.0 79.1 %copy-start.3 = (f32[3,64,128]{2,1,0:T(8,128)S(1)}, f32[3,64,128]{2,1,0:T(8,128)}, u32[]{:S(2)}) copy-start(f32[3,64,128]{2,1,0:T(8,128)} %param.9) | copy-start | bytes 294916
where the time goes:
time: 169 us
  blocking collectives  120 us (71%)
  waiting for transfers between devices  18.5 us (11%)
  matrix products  12.8 us (8%)
  starting transfers between devices  11.4 us (7%)
  local copies, waits for them, and re-layouts  4.01 us (2%)
    all_to_all x2, blocking collectives, sent_to_all(): return lax.all_to_all(copies, axis, split_axis=0, concat_axis=0, tiled=True)  59.9 us
    psum x4, blocking collectives, over_axes(): array = lax.psum(array, axis)  39.8 us
    all_to_all x1, blocking collectives, sent_and_summed(): lax.all_to_all(blocks, axis, split_axis=0, concat_axis=0, tiled=True)  19.9 us
    all_to_all x1, waiting for transfers between devices, sent_to_all(): return lax.all_to_all(copies, axis, split_axis=0, concat_axis=0, tiled=True)  18.5 us
    all_to_all x1, starting transfers between devices, sent_to_all(): return lax.all_to_all(copies, axis, split_axis=0, concat_axis=0, tiled=True)  11.4 us
    dot_general x1, matrix products, on_device(): jnp.einsum('td,mtc->dmc', inputs, cotangents, preferred_element_type=jnp....  8.65 us
  transfers between devices with their start and end apart: 1, of which 1 were waited for; matrix products, arithmetic and copies ran while one was open for 5% of the time, Pallas kernels for 0%

commit v1 on v0

--- a/solution.py
+++ b/solution.py
@@ -39,7 +39,7 @@
 
 def over_axes(array, axes):
     for axis in axes:
-        array = lax.psum(array, axis)
+        array = jnp.sum(lax.all_gather(array, axis), axis=0)
     return array
 
 

time: 169 us -> 178 us (1.053)
  blocking collectives: 120 us -> 97.1 us
  waiting for transfers between devices: 18.5 us -> 31.6 us
  local copies, waits for them, and re-layouts: 4.01 us -> 12.7 us
  starting transfers between devices: 11.4 us -> 17.8 us
  other arithmetic: 1.25 us -> 3.67 us
    psum x4 -> x0, blocking collectives: 39.8 us -> none  [over_axes(): array = lax.psum(array, axis)]
    unnamed x0 -> x4, blocking collectives: none -> 37.3 us
    all_to_all x1 -> x0, blocking collectives: 19.9 us -> none  [sent_and_summed(): lax.all_to_all(blocks, axis, split_axis=0, concat_axis=0, tiled=True)]
    all_to_all x0 -> x1, waiting for transfers between devices: none -> 13.1 us  [sent_and_summed(): lax.all_to_all(blocks, axis, split_axis=0, concat_axis=0, tiled=True)]
    unnamed x12 -> x32, local copies, waits for them, and re-layouts: 0.17 us -> 8.15 us
    all_to_all x0 -> x1, starting transfers between devices: none -> 6.46 us  [sent_and_summed(): lax.all_to_all(blocks, axis, split_axis=0, concat_axis=0, tiled=True)]
    reduce_sum x0 -> x4, other arithmetic: none -> 2.41 us  [over_axes(): array = jnp.sum(lax.all_gather(array, axis), axis=0)]
  transfers between devices with their start and end apart: 1 -> 2, of which waited for: 1 -> 2; matrix products, arithmetic and copies ran while one was open for 5% -> 5% of each run, Pallas kernels for 0% -> 0%
where the time goes in v1:
time: 178 us; the launch traced here: 177 us
  blocking collectives  97.1 us (55%)
  waiting for transfers between devices  31.6 us (18%)
  starting transfers between devices  17.8 us (10%)
  matrix products  12.8 us (7%)
  local copies, waits for them, and re-layouts  12.7 us (7%)
  other arithmetic  3.67 us (2%)
    all_to_all x2, blocking collectives, sent_to_all(): return lax.all_to_all(copies, axis, split_axis=0, concat_axis=0, tiled=True)  59.9 us
    unnamed x4, blocking collectives  37.3 us
    all_to_all x1, waiting for transfers between devices, sent_to_all(): return lax.all_to_all(copies, axis, split_axis=0, concat_axis=0, tiled=True)  18.5 us
    all_to_all x1, waiting for transfers between devices, sent_and_summed(): lax.all_to_all(blocks, axis, split_axis=0, concat_axis=0, tiled=True)  13.1 us
    all_to_all x1, starting transfers between devices, sent_to_all(): return lax.all_to_all(copies, axis, split_axis=0, concat_axis=0, tiled=True)  11.4 us
    dot_general x1, matrix products, on_device(): jnp.einsum('td,mtc->dmc', inputs, cotangents, preferred_element_type=jnp....  8.65 us
    unnamed x32, local copies, waits for them, and re-layouts  8.15 us
    all_to_all x1, starting transfers between devices, sent_and_summed(): lax.all_to_all(blocks, axis, split_axis=0, concat_axis=0, tiled=True)  6.46 us
  transfers between devices with their start and end apart: 2, of which 2 were waited for; matrix products, arithmetic and copies ran while one was open for 5% of the time, Pallas kernels for 0%

profile of v1, /device:TPU:32, one launch (start us, length us, event | category | flops | bytes accessed | tf_op | source)
XLA Modules:
  0.0 177.2 jit_solution(2339017363665454300)
XLA Ops:
  0.6 0.0 copy-start
  0.6 2.0 %broadcast_in_dim.9 = bf16[32,64,256]{2,1,0:T(8,128)(2,1)} broadcast(bf16[64,256]{1,0:T(8,128)(2,1)} %param.8), dimensions={1,2} | broadcast | bytes 1081344 | tf_op jit(solution)/shard_map/broadcast_in_dim | solution.py:21
  2.6 11.4 %all-to-all-start = ((bf16[32,64,256]{2,1,0:T(8,128)(2,1)}), bf16[32,64,256]{2,1,0:T(8,128)(2,1)S(1)}, u32[]{:S(2)}, u32[]{:S(2)}) async-start(bf16[32,64,256]{2,1,0:T(8,128)(2,1)} %broadcast_in_dim.9), calls=%async_computation | async-start | bytes 2097152 | tf_op jit(solution)/shard_map/all_to_all | solution.py:22
  14.0 0.0 copy-done
  14.0 8.6 %fusion = f32[2048,3,128]{2,0,1:T(8,128)} fusion(bf16[3,2048,128]{2,1,0:T(8,128)(2,1)S(1)} %copy-done, bf16[2048,2048]{1,0:T(8,128)(2,1)} %param.6), kind=kOutput, calls=%fused_computation | convolution fusion | flops 3221225472 | bytes 13107200 | tf_op jit(solution)/shard_map/td,mtc->dmc/dot_general | solution.py:48
  22.6 18.5 %all-to-all-done = bf16[32,64,256]{2,1,0:T(8,128)(2,1)S(1)} async-done(((bf16[32,64,256]{2,1,0:T(8,128)(2,1)}), bf16[32,64,256]{2,1,0:T(8,128)(2,1)S(1)}, u32[]{:S(2)}, u32[]{:S(2)}) %all-to-all-start) | async-done | bytes 1048608 | tf_op jit(solution)/shard_map/all_to_all | solution.py:22
  41.2 2.7 %fusion.6 = f32[3,128,256]{2,1,0:T(8,128)S(1)} fusion(bf16[2048,256,1]{1,0,2:T(8,128)(2,1)S(1)} %bitcast.46, f32[2048,3,128]{2,0,1:T(8,128)} %fusion), kind=kOutput, calls=%fused_computation.8 | convolution fusion | flops 403439616 | bytes 4587520 | tf_op jit(solution)/shard_map/dr,dmc->rmc/dot_general | solution.py:54
  43.8 0.1 copy-done.1
  44.0 0.0 copy-start.4
  44.0 0.0 copy-start.5
  44.0 0.0 copy-start.2
  44.0 0.0 copy-start.3
  44.1 0.6 fusion.4
  44.7 0.2 copy.27
  44.9 0.8 copy.28
  45.6 6.5 %all-to-all-start.1 = ((f32[32,8,3,128]{3,1,2,0:T(8,128)}), f32[32,8,3,128]{3,1,2,0:T(8,128)S(1)}, u32[]{:S(2)}, u32[]{:S(2)}) async-start(f32[32,8,3,128]{3,1,2,0:T(8,128)} %copy.28), calls=%async_computation.1 | async-start | bytes 786432 | tf_op jit(solution)/shard_map/all_to_all | solution.py:36
  52.1 0.0 copy-done.9
  52.1 0.6 dynamic-slice
  52.7 13.1 %all-to-all-done.1 = f32[32,8,3,128]{3,1,2,0:T(8,128)S(1)} async-done(((f32[32,8,3,128]{3,1,2,0:T(8,128)}), f32[32,8,3,128]{3,1,2,0:T(8,128)S(1)}, u32[]{:S(2)}, u32[]{:S(2)}) %all-to-all-start.1) | async-done | bytes 393248 | tf_op jit(solution)/shard_map/all_to_all | solution.py:36
  65.8 0.6 multiply_reduce_fusion
  66.4 1.4 dynamic-update-slice
  67.8 0.0 copy-done.8
  67.8 0.6 dynamic-slice.1
  68.4 14.9 %all-reduce = f32[8]{0:T(128)S(1)} all-reduce(f32[8]{0:T(128)S(1)} %dynamic-update-slice), channel_id=1, replica_groups=mesh['fs_0'=8,'fs_1'=4,'tp_0'=4,'tp_1'=2] {'fs_0'}, use_global_device_ids=true, to_apply=%add | all-reduce | flops 8 | bytes 64
  83.3 0.6 reduce_sum.56
  83.9 1.4 dynamic-update-slice.1
  85.3 0.0 copy-done.7
  85.3 0.6 dynamic-slice.2
  85.9 9.5 %all-reduce.1 = f32[4]{0:T(128)S(1)} all-reduce(f32[4]{0:T(128)S(1)} %dynamic-update-slice.1), channel_id=1, replica_groups=mesh['fs_0'=8,'fs_1'=4,'tp_0'=4,'tp_1'=2] {'fs_1'}, use_global_device_ids=true, to_apply=%add.1 | all-reduce | flops 4 | bytes 32
  95.4 0.6 reduce_sum.57
  96.0 1.4 dynamic-update-slice.2
  97.4 0.0 copy-done.6
  97.4 0.6 dynamic-slice.3
  98.0 10.5 %all-reduce.2 = f32[4]{0:T(128)S(1)} all-reduce(f32[4]{0:T(128)S(1)} %dynamic-update-slice.2), channel_id=1, replica_groups=mesh['fs_0'=8,'fs_1'=4,'tp_0'=4,'tp_1'=2] {'tp_0'}, use_global_device_ids=true, to_apply=%add.2 | all-reduce | flops 4 | bytes 32
  108.4 0.6 reduce_sum.58
  109.0 1.4 dynamic-update-slice.3
  110.4 2.4 %all-reduce.3 = f32[2]{0:T(128)S(1)} all-reduce(f32[2]{0:T(128)S(1)} %dynamic-update-slice.3), channel_id=1, replica_groups=mesh['fs_0'=8,'fs_1'=4,'tp_0'=4,'tp_1'=2] {'tp_1'}, use_global_device_ids=true, to_apply=%add.3 | all-reduce | flops 2 | bytes 16
  112.9 0.6 reduce_sum.59
  114.2 0.0 copy-done.4
  114.2 0.0 copy-done.5
  114.2 0.6 add_divide_fusion
  114.8 16.5 %all_to_all.20 = bf16[32,3,8,128]{3,2,1,0:T(8,128)(2,1)S(1)} all-to-all(bf16[32,3,8,128]{3,2,1,0:T(8,128)(2,1)S(1)} %broadcast_in_dim.10), channel_id=1, replica_groups=mesh['fs_0'=8,'fs_1'=4,'tp_0'=4,'tp_1'=2] {'fs_0','fs_1'}, dimensions={0} | all-to-all | bytes 393216 | tf_op jit(solution)/shard_map/all_to_all | solution.py:22
  131.3 0.0 copy-done.2
  131.3 0.0 copy-done.3
  131.3 0.8 fusion.13
  132.2 0.4 broadcast_in_dim.11
  132.5 43.4 %all_to_all.21 = bf16[32,3,64,128]{3,2,1,0:T(8,128)(2,1)S(1)} all-to-all(bf16[32,3,64,128]{3,2,1,0:T(8,128)(2,1)S(1)} %broadcast_in_dim.11), channel_id=1, replica_groups=mesh['fs_0'=8,'fs_1'=4,'tp_0'=4,'tp_1'=2] {'fs_0','fs_1'}, dimensions={0} | all-to-all | bytes 3145728 | tf_op jit(solution)/shard_map/all_to_all | solution.py:22
  175.9 1.3 copy.30
  (11 shorter events, 0.1 us)
Async XLA Ops:
  0.6 13.4 %copy-start = (bf16[3,2048,128]{2,1,0:T(8,128)(2,1)S(1)}, bf16[3,2048,128]{2,1,0:T(8,128)(2,1)}, u32[]{:S(2)}) copy-start(bf16[3,2048,128]{2,1,0:T(8,128)(2,1)} %param.7) | copy-start | bytes 4718596
  2.6 38.5 %all-to-all-start = ((bf16[32,64,256]{2,1,0:T(8,128)(2,1)}), bf16[32,64,256]{2,1,0:T(8,128)(2,1)S(1)}, u32[]{:S(2)}, u32[]{:S(2)}) async-start(bf16[32,64,256]{2,1,0:T(8,128)(2,1)} %broadcast_in_dim.9), calls=%async_computation | async-start | bytes 2097152 | tf_op jit(solution)/shard_map/all_to_all | solution.py:22
  41.2 2.8 %copy-start.1 = (f32[2048,3,128]{2,0,1:T(8,128)S(1)}, f32[2048,3,128]{2,0,1:T(8,128)}, u32[]{:S(2)}) copy-start(f32[2048,3,128]{2,0,1:T(8,128)} %fusion) | copy-start | bytes 9437188
  44.0 8.1 %copy-start.9 = (u32[256]{0:T(256)S(1)}, u32[256]{0:T(256)}, u32[]{:S(2)}) copy-start(u32[256]{0:T(256)} %constant.27) | copy-start | bytes 3076
  44.0 23.8 %copy-start.8 = (u32[256]{0:T(256)S(1)}, u32[256]{0:T(256)}, u32[]{:S(2)}) copy-start(u32[256]{0:T(256)} %constant.32) | copy-start | bytes 3076
  44.0 41.3 %copy-start.7 = (u32[256]{0:T(256)S(1)}, u32[256]{0:T(256)}, u32[]{:S(2)}) copy-start(u32[256]{0:T(256)} %constant.37) | copy-start | bytes 3076
  44.0 53.4 %copy-start.6 = (u32[256]{0:T(256)S(1)}, u32[256]{0:T(256)}, u32[]{:S(2)}) copy-start(u32[256]{0:T(256)} %constant.42) | copy-start | bytes 3076
  44.0 70.2 %copy-start.4 = (f32[3,8,128]{2,1,0:T(8,128)S(1)}, f32[3,8,128]{2,1,0:T(8,128)}, u32[]{:S(2)}) copy-start(f32[3,8,128]{2,1,0:T(8,128)} %param.11) | copy-start | bytes 36868
  44.0 70.2 %copy-start.5 = (f32[3,8,128]{2,1,0:T(8,128)S(1)}, f32[3,8,128]{2,1,0:T(8,128)}, u32[]{:S(2)}) copy-start(f32[3,8,128]{2,1,0:T(8,128)} %param.10) | copy-start | bytes 36868
  44.0 87.3 %copy-start.2 = (bf16[64,256]{1,0:T(8,128)(2,1)S(1)}, bf16[64,256]{1,0:T(8,128)(2,1)}, u32[]{:S(2)}) copy-start(bf16[64,256]{1,0:T(8,128)(2,1)} %param.8) | copy-start | bytes 98308
  44.0 87.3 %copy-start.3 = (f32[3,64,128]{2,1,0:T(8,128)S(1)}, f32[3,64,128]{2,1,0:T(8,128)}, u32[]{:S(2)}) copy-start(f32[3,64,128]{2,1,0:T(8,128)} %param.9) | copy-start | bytes 294916
  45.6 20.1 %all-to-all-start.1 = ((f32[32,8,3,128]{3,1,2,0:T(8,128)}), f32[32,8,3,128]{3,1,2,0:T(8,128)S(1)}, u32[]{:S(2)}, u32[]{:S(2)}) async-start(f32[32,8,3,128]{3,1,2,0:T(8,128)} %copy.28), calls=%async_computation.1 | async-start | bytes 786432 | tf_op jit(solution)/shard_map/all_to_all | solution.py:36
